TPU v7x, 512 devices: a whole 4x8x8 slice. The times are simulated.
512 devices in a mesh: sp: 64 (over z, y), tp: 8 (over x, core).
Axes of the slice: x: 4, y: 8, z: 8, core: 2. Of those that a mesh axis runs over, the one named last changes fastest.
Arguments:
- inner_pre: bfloat16 [24576, 4096], P('sp', 'tp'), may hold values from -6 to 6
- coeff_pre: bfloat16 [24576, 2, 1024], P('sp', None, 'tp'), may hold values from -6 to 6
- gate_pre: bfloat16 [24576, 4096], P('sp', 'tp'), may hold values from -6 to 6
- step_raw: bfloat16 [24576, 64], P('sp', 'tp'), may hold values from -2.5 to 2.5
- step_bias: float32 [64], P('tp'), may hold values from -3.3 to 0.8
- decay_log: float32 [64], P('tp'), may hold values from -8.5 to -3.5
- conv_inner: bfloat16 [4, 4096], P(None, 'tp'), may hold values from -3 to 3
- conv_coeff: bfloat16 [4, 2, 1024], P(None, None, 'tp'), may hold values from -3 to 3
- mixer_gain: float32 [4096], P('tp'), may hold values from 0.1 to 1.9
- out_weight: bfloat16 [4096, 2048], P('tp'), may hold values from -0.125 to 0.125
- residual: bfloat16 [24576, 2048], P('sp', 'tp'), may hold values from -12 to 12
- mlp_gain: float32 [2048], P('tp'), may hold values from 0.1 to 1.9
- up_weight: bfloat16 [2048, 8192], P('sp', 'tp'), may hold values from -0.125 to 0.125
- down_weight: bfloat16 [8192, 2048], P('tp', 'sp'), may hold values from -0.1875 to 0.1875
Outputs:
- layer_out: bfloat16 [24576, 2048], P('sp', 'tp')
All inputs are finite; a program needn't handle non-finite values.
Results may differ from a plain program's by a relative error of at most 0.02.
Values may be sent and summed in bfloat16 or wider, within the bound.
A program may use at most 64 MiB of HBM per device.

v0:
```python
import jax
import jax.numpy as jnp
from jax import lax
from jax.sharding import Mesh
from jax.sharding import PartitionSpec as P

D = 2048
INNER = 4096
HEAD_DIM = 64
GROUPS = 8
STATE = 128
BLOCK = 128
SP = ("sp_0", "sp_1")
eps_norm = 1e-05


def turned_gather(arrays, axis, dims):
    turned = [jnp.moveaxis(a, dim, 0) for a, dim in zip(arrays, dims)]
    both = jnp.concatenate([t.reshape(len(t), -1) for t in turned], axis=1)
    result, at, finished = (lax.all_gather(both, axis, axis=0, tiled=True), 0, [])
    for t, dim in zip(turned, dims):
        share = result[:, at : at + t[0].size].reshape(-1, *t.shape[1:])
        finished.append(jnp.moveaxis(share, 0, dim))
        at += t[0].size
    return tuple(finished)


def passed_along(block, axis, distance):
    devices = range(lax.axis_size(axis))
    route = [(i - distance, i) for i in devices if i - distance in devices]
    return lax.ppermute(block, axis, route)


def nothing_yet(array, identity):
    return jax.tree.map(
        lambda a, e: jnp.broadcast_to(jnp.asarray(e, a.dtype), a.shape), array, identity
    )


def carried_in(array, axes, combine, identity):
    before = start = nothing_yet(array, identity)
    so_far = array
    for axis in reversed(axes):
        size, index = (lax.axis_size(axis), lax.axis_index(axis))
        pieces = jax.tree.map(
            lambda part, kind: lax.all_gather(part.astype(kind), axis),
            so_far,
            (jnp.bfloat16, jnp.bfloat16),
        )
        inside, so_far = (start, start)
        for k in range(size):
            passed = k < index
            so_far = combine(
                so_far, jax.tree.map(lambda part, own: part[k].astype(own.dtype), pieces, array)
            )
            inside = jax.tree.map(lambda new, old: jnp.where(passed, new, old), so_far, inside)
        before = combine(inside, before)
    return before


def in_blocks(array, dim, size):
    before, after = (array.shape[:dim], array.shape[dim + 1 :])
    return jnp.moveaxis(array.reshape(*before, size, -1, *after), dim, 0)


def sent_and_summed(array, axis, dim):
    parts = in_blocks(array, dim, lax.axis_size(axis))
    arrived = lax.all_to_all(parts, axis, split_axis=0, concat_axis=0, tiled=True)
    return arrived.astype(jnp.float32).sum(axis=0)


def copy_for_each(array, axis):
    size = lax.axis_size(axis)
    return lax.all_to_all(
        jnp.broadcast_to(array[None], (size, *array.shape)), axis, 0, 0, tiled=True
    )


def of_everyone(array, axis):
    everything = copy_for_each(array, axis)
    return jnp.sum(everything, axis=0)


def laid_out(parts, dim):
    shape = list(parts.shape[1:])
    shape[dim] *= parts.shape[0]
    return jnp.moveaxis(parts, 0, dim).reshape(shape)


def gathered_copies(array, axis, dim):
    return laid_out(copy_for_each(array, axis), dim)


def causal_taps(history, current, weights):
    extended = jnp.concatenate([history, current], axis=0).astype(jnp.float32)
    length = current.shape[0]
    summed = extended[0:length] * weights[0].astype(jnp.float32)
    for offset in range(1, weights.shape[0]):
        summed = summed + extended[offset : offset + length] * weights[offset].astype(jnp.float32)
    return jax.nn.silu(summed)


def combine_states(first_part, second_part):
    decay_one, state_one = first_part
    decay_two, state_two = second_part
    return (decay_one * decay_two, state_one * decay_two[..., None, None] + state_two)


def shards(
    inner_pre,
    coeff_pre,
    gate_pre,
    step_raw,
    step_bias,
    decay_log,
    conv_inner,
    conv_coeff,
    mixer_gain,
    out_weight,
    residual,
    mlp_gain,
    up_weight,
    down_weight,
):
    up_whole, down_whole = turned_gather((up_weight, down_weight), SP, (0, 1))
    row_count = inner_pre.shape[0]
    edge_rows = conv_inner.shape[0] - 1
    inner_cols = inner_pre.shape[1]
    coeff_cols = coeff_pre.shape[2]
    tail_rows = jnp.concatenate(
        [
            inner_pre[row_count - edge_rows :],
            coeff_pre[row_count - edge_rows :].reshape(edge_rows, 2 * coeff_cols),
        ],
        axis=1,
    )
    arrived = passed_along(tail_rows, SP, 1)
    inner_act = causal_taps(arrived[:, :inner_cols], inner_pre, conv_inner)
    coeff_act = causal_taps(
        arrived[:, inner_cols:].reshape(edge_rows, 2, coeff_cols), coeff_pre, conv_coeff
    )
    heads_here = step_raw.shape[1]
    groups_here = coeff_cols // STATE
    per_group = heads_here // groups_here
    blocks = row_count // BLOCK
    in_coeff = coeff_act[:, 0].reshape(blocks, BLOCK, groups_here, STATE)
    out_coeff = coeff_act[:, 1].reshape(blocks, BLOCK, groups_here, STATE)
    step_size = jax.nn.softplus(step_raw.astype(jnp.float32) + step_bias)
    log_step = (-step_size * jnp.exp(decay_log)).reshape(blocks, BLOCK, groups_here, per_group)
    values = (
        inner_act.reshape(blocks, BLOCK, groups_here, per_group, HEAD_DIM)
        * step_size.reshape(blocks, BLOCK, groups_here, per_group)[..., None]
    )
    log_cumul = jnp.cumsum(log_step, axis=1)
    position = jnp.arange(BLOCK)
    causal_mask = (position[:, None] >= position[None, :])[None, :, :, None, None]
    log_gaps = log_cumul[:, :, None] - log_cumul[:, None, :]
    within = jnp.where(causal_mask, jnp.exp(jnp.where(causal_mask, log_gaps, 0.0)), 0.0)
    scores = jnp.einsum("blgn,bsgn->blsg", out_coeff, in_coeff)
    inside = jnp.einsum("blsg,blsgh,bsghp->blghp", scores, within, values)
    to_end = jnp.exp(log_cumul[:, -1:] - log_cumul)
    block_states = jnp.einsum("blgn,blgh,blghp->bghpn", in_coeff, to_end, values)
    block_logs = log_cumul[:, -1]
    block_ends = jnp.cumsum(block_logs, axis=0)
    block_starts = block_ends - block_logs
    block_index = jnp.arange(blocks)
    before = (block_index[None, :] < block_index[:, None])[:, :, None, None]
    log_spans = block_starts[:, None] - block_ends[None, :]
    block_links = jnp.where(before, jnp.exp(jnp.where(before, log_spans, 0.0)), 0.0)
    entering = jnp.einsum("nmgh,mghpk->nghpk", block_links, block_states)
    own_state = jnp.einsum(
        "mgh,mghpk->ghpk", jnp.exp(block_ends[-1][None] - block_ends), block_states
    )
    own_decay = jnp.exp(block_ends[-1])
    identity = (jnp.ones_like(own_decay), jnp.zeros_like(own_state))
    enter_decay, enter_state = carried_in((own_decay, own_state), SP, combine_states, identity)
    entering = entering + jnp.exp(block_starts)[..., None, None] * enter_state[None]
    carried = jnp.einsum("blgn,bghpn,blgh->blghp", out_coeff, entering, jnp.exp(log_cumul))
    scan_out = (inside + carried).reshape(row_count, inner_cols)
    gated = scan_out * jax.nn.silu(gate_pre.astype(jnp.float32))
    grouped = gated.reshape(row_count, groups_here, INNER // GROUPS)
    grouped = grouped * lax.rsqrt(jnp.mean(grouped * grouped, axis=2, keepdims=True) + eps_norm)
    mixed_rows = (grouped.reshape(row_count, inner_cols) * mixer_gain).astype(jnp.bfloat16)
    projected = sent_and_summed(
        jnp.dot(mixed_rows, out_weight, preferred_element_type=jnp.float32).astype(jnp.bfloat16),
        "tp",
        1,
    )
    first_sum = (residual.astype(jnp.float32) + projected).astype(jnp.bfloat16)
    first_wide = first_sum.astype(jnp.float32)
    squares = of_everyone(jnp.sum(first_wide * first_wide, axis=1), "tp")
    normed = (first_wide * lax.rsqrt(squares / D + eps_norm)[:, None] * mlp_gain).astype(
        jnp.bfloat16
    )
    whole_rows = gathered_copies(normed, "tp", 1)
    hidden = jnp.dot(whole_rows, up_whole, preferred_element_type=jnp.float32)
    active = jnp.square(jax.nn.relu(hidden)).astype(jnp.bfloat16)
    partials = jnp.dot(active, down_whole, preferred_element_type=jnp.float32)
    lowered = sent_and_summed(partials.astype(jnp.bfloat16), "tp", 1)
    return (first_wide + lowered).astype(jnp.bfloat16)


def solution(mesh):
    split = Mesh(mesh.devices.reshape(8, 8, mesh.shape["tp"]), ("sp_0", "sp_1", "tp"))
    return jax.shard_map(
        shards,
        mesh=split,
        in_specs=(
            P(SP, "tp"),
            P(SP, None, "tp"),
            P(SP, "tp"),
            P(SP, "tp"),
            P("tp"),
            P("tp"),
            P(None, "tp"),
            P(None, None, "tp"),
            P("tp"),
            P("tp", None),
            P(SP, "tp"),
            P("tp"),
            P(SP, "tp"),
            P("tp", SP),
        ),
        out_specs=P(SP, "tp"),
        check_vma=False,
    )
```

profile of v0, /device:TPU:1, one launch (start us, length us, event | category | flops | bytes accessed | tf_op | source)
XLA Modules:
  0.0 260.9 jit_solution(793769002312632758)
XLA Ops:
  6.5 0.9 slice.176
  7.4 0.7 slice_bitcast_fusion.8
  8.1 0.8 copy.96
  8.9 4.0 %collective-permute-start = (bf16[3,768]{0,1:T(8,128)(2,1)}, bf16[3,768]{0,1:T(8,128)(2,1)S(1)}, u32[]{:S(2)}, u32[]{:S(2)}) collective-permute-start(bf16[3,768]{0,1:T(8,128)(2,1)} %copy.96), channel_id=1, source_target_pairs={{0,8},{8,16},{16,24},{24,32},{32,40},{40,48},{48,56},{56,64},{64,7... | collective-permute-start | bytes 13832 | tf_op jit(solution)/shard_map/ppermute | solution.py:31
  13.0 0.7 exp.65
  13.6 0.8 fusion.70
  14.7 0.6 slice_bitcast_fusion.16
  15.3 0.6 bitcast_subtract_fusion
  15.9 0.8 slice_convert_fusion.3
  16.7 1.3 bitcast_convert_fusion.3
  18.1 0.7 fusion.99
  19.0 0.7 copy.106
  19.7 0.7 copy.122
  21.1 1.9 divide_multiply_fusion
  23.0 1.5 reshape.593
  24.6 1.1 maximum_convert_fusion.1
  25.8 0.6 divide_multiply_fusion.1
  26.7 1.1 broadcast_multiply_fusion
  28.9 0.7 convert_element_type.466
  29.7 13.0 %all_gather.21 = bf16[8,1,8]{2,1,0:T(2,128)(2,1)S(1)} all-gather(bf16[1,1,8]{2,1,0:T(2,128)(2,1)S(1)} %copy-done.52), channel_id=1, replica_groups=mesh['sp_0'=8,'sp_1'=8,'tp'=8] {'sp_1'}, dimensions={0}, use_global_device_ids=true | all-gather | bytes 144 | tf_op jit(solution)/shard_map/all_gather | solution.py:46
  43.2 26.5 %all-gather.9.cloned.1.call-done = bf16[64,64,128]{2,1,0:T(8,128)(2,1)} async-done(((bf16[8,64,128]{2,1,0:T(8,128)(2,1)}), bf16[64,64,128]{2,1,0:T(8,128)(2,1)}) %all-gather.9.cloned.1.call-update) | async-done | bytes 1048592 | tf_op jit(solution)/shard_map/all_gather | solution.py:46
  69.7 2.2 fusion.64
  72.1 0.7 pad_maximum_fusion
  72.8 0.7 copy.100
  73.5 0.7 copy.112
  74.2 0.7 copy.125
  74.8 0.7 copy.110
  75.6 1.0 copy.115
  76.6 13.6 %all_gather.22 = bf16[8,1,8]{2,1,0:T(2,128)(2,1)S(1)} all-gather(bf16[1,1,8]{2,1,0:T(2,128)(2,1)S(1)} %multiply_convert_fusion.3), channel_id=1, replica_groups=mesh['sp_0'=8,'sp_1'=8,'tp'=8] {'sp_0'}, dimensions={0}, use_global_device_ids=true | all-gather | bytes 144 | tf_op jit(solution)/shard_map/all_gather | solution.py:46
  90.2 0.6 iota_compare_fusion.1
  90.8 0.6 iota_compare_fusion
  91.9 0.6 fusion.83
  92.8 0.8 copy.98
  93.7 2.8 %fusion.17 = f32[3,128,1,8,64]{1,4,3,0,2:T(8,128)} fusion(bf16[3,128,8,64]{1,0,3,2:T(4,128)(2,1)} %get-tuple-element.8, f32[3,128,8]{1,2,0:T(8,128)} %copy.100, f32[3,128,128]{2,1,0:T(8,128)} %copy.98, pred[128,128]{1,0:T(8,128)(4,1)} %iota_compare_fusion), kind=kOutput, calls=%fused_computation.20 | convolution fusion | flops 51904512 | bytes 1404928 | tf_op jit(solution)/shard_map/blsg,blsgh,bsghp->blghp/dot_general | solution.py:160
  96.6 16.6 %all-gather.5.cloned.1.call-done = bf16[8,1,8,64,128]{4,3,2,1,0:T(8,128)(2,1)} async-done(((bf16[1,1,8,64,128]{4,3,2,1,0:T(8,128)(2,1)}), bf16[8,1,8,64,128]{4,3,2,1,0:T(8,128)(2,1)}) %all-gather.5.cloned.1.call-update) | async-done | bytes 1048592 | tf_op jit(solution)/shard_map/all_gather | solution.py:46
  113.4 2.0 fusion.63
  115.4 0.6 fusion.16
  116.8 0.5 copy.114
  117.8 1.2 convolution_convert_fusion
  119.1 29.9 %all_to_all.21 = bf16[8,384,256]{2,1,0:T(8,128)(2,1)S(1)} all-to-all(bf16[8,384,256]{2,1,0:T(8,128)(2,1)S(1)} %bitcast.260), channel_id=1, replica_groups=mesh['sp_0'=8,'sp_1'=8,'tp'=8] {'tp'}, dimensions={0} | all-to-all | bytes 3145728 | tf_op jit(solution)/shard_map/all_to_all | solution.py:68
  149.3 0.7 copy-done.12
  150.1 8.0 %all_to_all.22 = f32[8,1,384]{2,1,0:T(1,128)S(1)} all-to-all(f32[8,1,384]{2,1,0:T(1,128)S(1)} %broadcast_in_dim.53), channel_id=1, replica_groups=mesh['sp_0'=8,'sp_1'=8,'tp'=8] {'tp'}, dimensions={0} | all-to-all | bytes 24576 | tf_op jit(solution)/shard_map/all_to_all | solution.py:74
  158.7 24.4 %all_to_all.23 = bf16[8,384,256]{1,2,0:T(8,128)(2,1)} all-to-all(bf16[8,384,256]{1,2,0:T(8,128)(2,1)S(1)} %broadcast_in_dim.54), channel_id=1, replica_groups=mesh['sp_0'=8,'sp_1'=8,'tp'=8] {'tp'}, dimensions={0} | all-to-all | bytes 3145728 | tf_op jit(solution)/shard_map/all_to_all | solution.py:74
  183.1 34.8 %all-gather.7.cloned.1.call-done = bf16[2048,2048]{1,0:T(8,128)(2,1)} async-done(((bf16[32,2048]{1,0:T(8,128)(2,1)}), bf16[2048,2048]{1,0:T(8,128)(2,1)}) %all-gather.7.cloned.1.call-update) | async-done | bytes 8388624 | tf_op jit(solution)/shard_map/all_gather | solution.py:20
  217.9 8.5 %fusion.4 = bf16[384,2048]{1,0:T(8,128)(2,1)} fusion(bf16[2048,2048]{1,0:T(8,128)(2,1)} %all-gather.7.cloned.1.call-done, bf16[384,2048]{0,1:T(8,128)(2,1)} %bitcast.270), kind=kOutput, calls=%fused_computation.6 | convolution fusion | flops 3223191552 | bytes 11534336 | tf_op jit(solution)/shard_map/dot_general | solution.py:198
  226.4 1.5 copy.160
  227.9 25.5 %all_to_all.24 = bf16[8,384,256]{2,1,0:T(8,128)(2,1)S(1)} all-to-all(bf16[8,384,256]{2,1,0:T(8,128)(2,1)S(1)} %bitcast.261), channel_id=1, replica_groups=mesh['sp_0'=8,'sp_1'=8,'tp'=8] {'tp'}, dimensions={0} | all-to-all | bytes 3145728 | tf_op jit(solution)/shard_map/all_to_all | solution.py:68
  253.7 0.7 fusion.47
  (156 shorter events, 6.5 us)
Async XLA Ops:
  6.5 111.3 %copy-start = (bf16[512,2048]{1,0:T(8,128)(2,1)S(1)}, bf16[512,2048]{1,0:T(8,128)(2,1)}, u32[]{:S(2)}) copy-start(bf16[512,2048]{1,0:T(8,128)(2,1)} %param.23) | copy-start | bytes 6291460
  6.5 12.3 %copy-start.7 = (bf16[384,512]{1,0:T(8,128)(2,1)S(1)}, bf16[384,512]{1,0:T(8,128)(2,1)}, u32[]{:S(2)}) copy-start(bf16[384,512]{1,0:T(8,128)(2,1)} %param.14) | copy-start | bytes 1179652
  6.5 63.2 %all-gather.9.cloned.1.call-start = ((), (), s32[]{:S(2)}) async-start(), calls=%async_computation.6 | async-start | bytes 1179648 | tf_op jit(solution)/shard_map/all_gather | solution.py:46
  8.9 11.5 %collective-permute-start = (bf16[3,768]{0,1:T(8,128)(2,1)}, bf16[3,768]{0,1:T(8,128)(2,1)S(1)}, u32[]{:S(2)}, u32[]{:S(2)}) collective-permute-start(bf16[3,768]{0,1:T(8,128)(2,1)} %copy.96), channel_id=1, source_target_pairs={{0,8},{8,16},{16,24},{24,32},{32,40},{40,48},{48,56},{56,64},{64,7... | collective-permute-start | bytes 13832 | tf_op jit(solution)/shard_map/ppermute | solution.py:31
  14.7 4.1 %copy-start.16 = (f32[3,1,8]{2,1,0:T(1,128)}, f32[3,1,8]{2,1,0:T(1,128)S(1)}, u32[]{:S(2)}) copy-start(f32[3,1,8]{2,1,0:T(1,128)S(1)} %fusion.75) | copy-start | bytes 292
  23.0 2.7 %copy-start.35 = (f32[2,128]{1,0:T(2,128)S(1)}, f32[2,128]{1,0:T(2,128)}, u32[]{:S(2)}) copy-start(f32[2,128]{1,0:T(2,128)} %get-tuple-element.37) | copy-start | bytes 3076
  23.0 2.7 %copy-start.36 = (f32[2,128]{1,0:T(2,128)S(1)}, f32[2,128]{1,0:T(2,128)}, u32[]{:S(2)}) copy-start(f32[2,128]{1,0:T(2,128)} %get-tuple-element.38) | copy-start | bytes 3076
  23.0 2.7 %copy-start.37 = (f32[2,128]{1,0:T(2,128)S(1)}, f32[2,128]{1,0:T(2,128)}, u32[]{:S(2)}) copy-start(f32[2,128]{1,0:T(2,128)} %get-tuple-element.39) | copy-start | bytes 3076
  23.0 2.7 %copy-start.38 = (f32[2,128]{1,0:T(2,128)S(1)}, f32[2,128]{1,0:T(2,128)}, u32[]{:S(2)}) copy-start(f32[2,128]{1,0:T(2,128)} %get-tuple-element.40) | copy-start | bytes 3076
  28.1 43.9 %copy-start.14 = (bf16[1024,32]{0,1:T(8,128)(2,1)S(1)}, bf16[1024,32]{0,1:T(8,128)(2,1)}, u32[]{:S(2)}) copy-start(bf16[1024,32]{0,1:T(8,128)(2,1)} %param.27) | copy-start | bytes 196612
  28.2 43.9 %copy-start.15 = (bf16[32,1024]{1,0:T(8,128)(2,1)S(1)}, bf16[32,1024]{1,0:T(8,128)(2,1)}, u32[]{:S(2)}) copy-start(bf16[32,1024]{1,0:T(8,128)(2,1)} %param.26) | copy-start | bytes 196612
  28.2 44.6 %copy-start.17 = (f32[3,1,8]{2,1,0:T(1,128)S(1)}, f32[3,1,8]{2,1,0:T(1,128)}, u32[]{:S(2)}) copy-start(f32[3,1,8]{2,1,0:T(1,128)} %copy-done.16) | copy-start | bytes 292
  28.2 45.3 %copy-start.19 = (f32[3,1,1,8]{3,2,1,0:T(1,128)S(1)}, f32[3,1,1,8]{3,2,1,0:T(1,128)}, u32[]{:S(2)}) copy-start(f32[3,1,1,8]{3,2,1,0:T(1,128)} %copy-done.18) | copy-start | bytes 292
  28.2 46.0 %copy-start.20 = (f32[3,1,1,8]{3,2,1,0:T(1,128)S(1)}, f32[3,1,1,8]{3,2,1,0:T(1,128)}, u32[]{:S(2)}) copy-start(f32[3,1,1,8]{3,2,1,0:T(1,128)} %get-tuple-element.13) | copy-start | bytes 292
  28.2 47.3 %copy-start.6 = (f32[3,128,8]{2,1,0:T(8,128)S(1)}, f32[3,128,8]{2,1,0:T(8,128)}, u32[]{:S(2)}) copy-start(f32[3,128,8]{2,1,0:T(8,128)} %get-tuple-element.11) | copy-start | bytes 36868
  28.7 46.9 %copy-start.8 = (bf16[384,512]{1,0:T(8,128)(2,1)S(1)}, bf16[384,512]{1,0:T(8,128)(2,1)}, u32[]{:S(2)}) copy-start(bf16[384,512]{1,0:T(8,128)(2,1)} %param.16) | copy-start | bytes 1179652
  29.6 62.9 %copy-start.3 = (f32[384,1,128]{2,1,0:T(1,128)S(1)}, f32[384,1,128]{2,1,0:T(1,128)}, u32[]{:S(2)}) copy-start(f32[384,1,128]{2,1,0:T(1,128)} %copy-done.2) | copy-start | bytes 589828
  29.6 83.6 %all-gather.5.cloned.1.call-start = ((), (), s32[]{:S(2)}) async-start(), calls=%async_computation.4 | async-start | bytes 1179648 | tf_op jit(solution)/shard_map/all_gather | solution.py:46
  43.2 49.5 %copy-start.33 = (f32[8]{0:T(128)}, f32[8]{0:T(128)S(1)}, u32[]{:S(2)}) copy-start(f32[8]{0:T(128)S(1)} %get-tuple-element.25) | copy-start | bytes 100
  43.2 49.5 %copy-start.21 = (f32[8]{0:T(128)}, f32[8]{0:T(128)S(1)}, u32[]{:S(2)}) copy-start(f32[8]{0:T(128)S(1)} %get-tuple-element.27) | copy-start | bytes 100
  43.2 49.5 %copy-start.23 = (f32[8]{0:T(128)}, f32[8]{0:T(128)S(1)}, u32[]{:S(2)}) copy-start(f32[8]{0:T(128)S(1)} %get-tuple-element.28) | copy-start | bytes 100
  43.2 49.5 %copy-start.25 = (f32[8]{0:T(128)}, f32[8]{0:T(128)S(1)}, u32[]{:S(2)}) copy-start(f32[8]{0:T(128)S(1)} %get-tuple-element.29) | copy-start | bytes 100
  43.2 49.5 %copy-start.27 = (f32[8]{0:T(128)}, f32[8]{0:T(128)S(1)}, u32[]{:S(2)}) copy-start(f32[8]{0:T(128)S(1)} %get-tuple-element.30) | copy-start | bytes 100
  43.2 49.5 %copy-start.29 = (f32[8]{0:T(128)}, f32[8]{0:T(128)S(1)}, u32[]{:S(2)}) copy-start(f32[8]{0:T(128)S(1)} %get-tuple-element.31) | copy-start | bytes 100
  43.2 49.5 %copy-start.31 = (f32[8]{0:T(128)}, f32[8]{0:T(128)S(1)}, u32[]{:S(2)}) copy-start(f32[8]{0:T(128)S(1)} %get-tuple-element.32) | copy-start | bytes 100
  72.0 145.9 %all-gather.7.cloned.1.call-start = ((), (), s32[]{:S(2)}) async-start(), calls=%async_computation.5 | async-start | bytes 8519680 | tf_op jit(solution)/shard_map/all_gather | solution.py:20
  93.6 19.6 %copy-start.1 = (bf16[64,64,128]{2,1,0:T(8,128)(2,1)S(1)}, bf16[64,64,128]{2,1,0:T(8,128)(2,1)}, u32[]{:S(2)}) copy-start(bf16[64,64,128]{2,1,0:T(8,128)(2,1)} %all-gather.9.cloned.1.call-done) | copy-start | bytes 3145732
  93.6 19.6 %copy-start.22 = (f32[8]{0:T(128)S(1)}, f32[8]{0:T(128)}, u32[]{:S(2)}) copy-start(f32[8]{0:T(128)} %copy-done.21) | copy-start | bytes 100
  93.6 19.6 %copy-start.24 = (f32[8]{0:T(128)S(1)}, f32[8]{0:T(128)}, u32[]{:S(2)}) copy-start(f32[8]{0:T(128)} %copy-done.23) | copy-start | bytes 100
  93.6 19.6 %copy-start.26 = (f32[8]{0:T(128)S(1)}, f32[8]{0:T(128)}, u32[]{:S(2)}) copy-start(f32[8]{0:T(128)} %copy-done.25) | copy-start | bytes 100
  93.6 19.6 %copy-start.28 = (f32[8]{0:T(128)S(1)}, f32[8]{0:T(128)}, u32[]{:S(2)}) copy-start(f32[8]{0:T(128)} %copy-done.27) | copy-start | bytes 100
  93.6 19.6 %copy-start.30 = (f32[8]{0:T(128)S(1)}, f32[8]{0:T(128)}, u32[]{:S(2)}) copy-start(f32[8]{0:T(128)} %copy-done.29) | copy-start | bytes 100
  93.6 19.6 %copy-start.32 = (f32[8]{0:T(128)S(1)}, f32[8]{0:T(128)}, u32[]{:S(2)}) copy-start(f32[8]{0:T(128)} %copy-done.31) | copy-start | bytes 100
  93.6 19.6 %copy-start.34 = (f32[8]{0:T(128)S(1)}, f32[8]{0:T(128)}, u32[]{:S(2)}) copy-start(f32[8]{0:T(128)} %copy-done.33) | copy-start | bytes 100
  93.6 19.6 %copy-start.43 = (f32[8]{0:T(128)S(1)}, f32[8]{0:T(128)}, u32[]{:S(2)}) copy-start(f32[8]{0:T(128)} %get-tuple-element.17) | copy-start | bytes 100
  93.6 19.6 %copy-start.44 = (f32[8]{0:T(128)S(1)}, f32[8]{0:T(128)}, u32[]{:S(2)}) copy-start(f32[8]{0:T(128)} %get-tuple-element.18) | copy-start | bytes 100
  93.7 19.6 %copy-start.45 = (f32[8]{0:T(128)S(1)}, f32[8]{0:T(128)}, u32[]{:S(2)}) copy-start(f32[8]{0:T(128)} %get-tuple-element.19) | copy-start | bytes 100
  93.7 19.6 %copy-start.46 = (f32[8]{0:T(128)S(1)}, f32[8]{0:T(128)}, u32[]{:S(2)}) copy-start(f32[8]{0:T(128)} %get-tuple-element.20) | copy-start | bytes 100
  93.7 19.6 %copy-start.47 = (f32[8]{0:T(128)S(1)}, f32[8]{0:T(128)}, u32[]{:S(2)}) copy-start(f32[8]{0:T(128)} %get-tuple-element.21) | copy-start | bytes 100
  93.7 19.6 %copy-start.48 = (f32[8]{0:T(128)S(1)}, f32[8]{0:T(128)}, u32[]{:S(2)}) copy-start(f32[8]{0:T(128)} %get-tuple-element.22) | copy-start | bytes 100
  93.7 19.6 %copy-start.49 = (f32[8]{0:T(128)S(1)}, f32[8]{0:T(128)}, u32[]{:S(2)}) copy-start(f32[8]{0:T(128)} %get-tuple-element.23) | copy-start | bytes 100
  93.7 19.6 %copy-start.50 = (f32[8]{0:T(128)S(1)}, f32[8]{0:T(128)}, u32[]{:S(2)}) copy-start(f32[8]{0:T(128)} %get-tuple-element.24) | copy-start | bytes 100
  93.7 19.6 %copy-start.53 = (f32[8]{0:T(128)S(1)}, f32[8]{0:T(128)}, u32[]{:S(2)}) copy-start(f32[8]{0:T(128)} %fusion.85) | copy-start | bytes 100
  96.6 18.8 %copy-start.40 = (f32[3,8]{0,1:T(8,128)S(1)}, f32[3,8]{0,1:T(8,128)}, u32[]{:S(2)}) copy-start(f32[3,8]{0,1:T(8,128)} %copy.112) | copy-start | bytes 292
  96.6 18.8 %copy-start.41 = (f32[3,8]{0,1:T(8,128)S(1)}, f32[3,8]{0,1:T(8,128)}, u32[]{:S(2)}) copy-start(f32[3,8]{0,1:T(8,128)} %copy.110) | copy-start | bytes 292
  96.6 18.9 %copy-start.42 = (f32[3,1,1,8]{0,3,2,1:T(8,128)S(1)}, f32[3,1,1,8]{0,3,2,1:T(8,128)}, u32[]{:S(2)}) copy-start(f32[3,1,1,8]{0,3,2,1:T(8,128)} %copy.125) | copy-start | bytes 292
  96.6 18.9 %copy-start.55 = (pred[3,3]{1,0:T(4,128)(4,1)S(1)}, pred[3,3]{1,0:T(4,128)(4,1)}, u32[]{:S(2)}) copy-start(pred[3,3]{1,0:T(4,128)(4,1)} %iota_compare_fusion.1) | copy-start | bytes 31
  149.0 9.2 %copy-start.51 = (f32[256]{0:T(256)S(1)}, f32[256]{0:T(256)}, u32[]{:S(2)}) copy-start(f32[256]{0:T(256)} %param.25) | copy-start | bytes 3076
  (13 other events, 18.7 us)
Sparse Core Ops, SparseCore 0:
  29.7 39.9 all-gather.8
  72.1 41.0 all-gather.4
  116.3 101.5 all-gather.6
where the time goes:
time: 262 us; the launch traced here: 261 us
  blocking collectives  115 us (44%)
  waiting for transfers between devices  78 us (30%)
  other arithmetic  20.3 us (8%)
  local copies, waits for them, and re-layouts  15.8 us (6%)
  matrix products  14.2 us (5%)
  between operations  14 us (5%)
  starting transfers between devices  4.1 us (2%)
    all_to_all x2, blocking collectives, sent_and_summed(): lax.all_to_all(parts, axis, split_axis=0, concat_axis=0, tiled=True)  55.5 us
    all_gather x2, waiting for transfers between devices, carried_in(): lax.all_gather(part.astype(kind), axis)  43.1 us
    all_gather x1, waiting for transfers between devices, turned_gather(): lax.all_gather(both, axis, axis=0, tiled=True)  34.8 us
    all_to_all x2, blocking collectives, copy_for_each(): lax.all_to_all(jnp.broadcast_to(array[None], (size, *array.shape)), axis,...  32.4 us
    all_gather x2, blocking collectives, carried_in(): lax.all_gather(part.astype(kind), axis)  26.6 us
    dot_general x1, matrix products, shards(): partials = jnp.dot(active, down_whole, preferred_element_type=jnp.float32)  8.49 us
  transfers between devices with their start and end apart: 4, of which 3 were waited for; matrix products, arithmetic and copies ran while one was open for 9% of the time, Pallas kernels for 0%

commit v1 on v0

--- a/solution.py
+++ b/solution.py
@@ -17,7 +17,13 @@
 def turned_gather(arrays, axis, dims):
     turned = [jnp.moveaxis(a, dim, 0) for a, dim in zip(arrays, dims)]
     both = jnp.concatenate([t.reshape(len(t), -1) for t in turned], axis=1)
-    result, at, finished = (lax.all_gather(both, axis, axis=0, tiled=True), 0, [])
+    result, at, finished = (
+        jnp.concatenate(
+            lax.all_to_all(jnp.stack([both] * lax.axis_size(axis)), axis, 0, 0), axis=0
+        ),
+        0,
+        [],
+    )
     for t, dim in zip(turned, dims):
         share = result[:, at : at + t[0].size].reshape(-1, *t.shape[1:])
         finished.append(jnp.moveaxis(share, 0, dim))

time: 262 us -> 440 us (1.68)
  the two profiles are of different devices: /device:TPU:1 before, /device:TPU:24 now
where the time goes in v1:
time: 440 us; the launch traced here: 439 us
  blocking collectives  299 us (68%)
  waiting for transfers between devices  65.1 us (15%)
  other arithmetic  19.7 us (4%)
  local copies, waits for them, and re-layouts  17.8 us (4%)
  matrix products  14.2 us (3%)
  between operations  14 us (3%)
  starting transfers between devices  9.36 us (2%)
    all_to_all x1, blocking collectives, turned_gather(): lax.all_to_all(jnp.stack([both] * lax.axis_size(axis)), axis, 0, 0)  211 us
    all_to_all x2, blocking collectives, sent_and_summed(): lax.all_to_all(parts, axis, split_axis=0, concat_axis=0, tiled=True)  49.7 us
    all_gather x2, waiting for transfers between devices, carried_in(): lax.all_gather(part.astype(kind), axis)  43.8 us
    all_gather x2, blocking collectives, carried_in(): lax.all_gather(part.astype(kind), axis)  30.4 us
    all_to_all x1, waiting for transfers between devices, copy_for_each(): lax.all_to_all(jnp.broadcast_to(array[None], (size, *array.shape)), axis,...  21.3 us
  transfers between devices with their start and end apart: 4, of which 3 were waited for; matrix products, arithmetic and copies ran while one was open for 4% of the time, Pallas kernels for 0%

profile of v1, /device:TPU:24, one launch (start us, length us, event | category | flops | bytes accessed | tf_op | source)
XLA Modules:
  0.0 439.2 jit_solution(15716794392138778103)
XLA Ops:
  6.5 0.8 slice_bitcast_fusion.8
  7.4 0.7 slice.176
  8.1 0.8 copy.96
  8.9 4.7 %collective-permute-start = (bf16[3,768]{0,1:T(8,128)(2,1)}, bf16[3,768]{0,1:T(8,128)(2,1)S(1)}, u32[]{:S(2)}, u32[]{:S(2)}) collective-permute-start(bf16[3,768]{0,1:T(8,128)(2,1)} %copy.96), channel_id=1, source_target_pairs={{0,8},{8,16},{16,24},{24,32},{32,40},{40,48},{48,56},{56,64},{64,7... | collective-permute-start | bytes 13832 | tf_op jit(solution)/shard_map/ppermute | solution.py:37
  13.6 0.7 exp.65
  14.3 0.8 fusion.70
  15.4 0.6 bitcast_subtract_fusion
  16.5 0.8 slice_convert_fusion.3
  17.4 1.3 bitcast_convert_fusion.3
  18.7 0.7 fusion.99
  19.7 0.7 copy.106
  20.4 0.7 copy.122
  21.7 1.9 divide_multiply_fusion
  23.6 1.5 reshape.598
  25.2 1.1 maximum_convert_fusion.1
  26.4 0.6 divide_multiply_fusion.1
  27.4 1.1 broadcast_multiply_fusion
  28.8 0.7 copy-done.9
  30.0 0.7 convert_element_type.466
  30.8 13.4 %all_gather.18 = bf16[8,1,8]{2,1,0:T(2,128)(2,1)S(1)} all-gather(bf16[1,1,8]{2,1,0:T(2,128)(2,1)S(1)} %copy-done.37), channel_id=1, replica_groups=mesh['sp_0'=8,'sp_1'=8,'tp'=8] {'sp_1'}, dimensions={0}, use_global_device_ids=true | all-gather | bytes 144 | tf_op jit(solution)/shard_map/all_gather | solution.py:52
  44.7 29.1 %all-gather.6.cloned.1.call-done = bf16[64,64,128]{2,1,0:T(8,128)(2,1)} async-done(((bf16[8,64,128]{2,1,0:T(8,128)(2,1)}), bf16[64,64,128]{2,1,0:T(8,128)(2,1)}) %all-gather.6.cloned.1.call-update) | async-done | bytes 1048592 | tf_op jit(solution)/shard_map/all_gather | solution.py:52
  73.9 2.3 fusion.64
  76.1 0.7 copy.100
  76.8 0.9 copy.115
  77.8 0.7 copy.112
  78.5 0.7 copy.110
  79.1 0.7 copy.125
  79.9 17.1 %all_gather.19 = bf16[8,1,8]{2,1,0:T(2,128)(2,1)S(1)} all-gather(bf16[1,1,8]{2,1,0:T(2,128)(2,1)S(1)} %multiply_convert_fusion.3), channel_id=1, replica_groups=mesh['sp_0'=8,'sp_1'=8,'tp'=8] {'sp_0'}, dimensions={0}, use_global_device_ids=true | all-gather | bytes 144 | tf_op jit(solution)/shard_map/all_gather | solution.py:52
  97.5 0.6 iota_compare_fusion
  98.1 0.6 fusion.85
  98.7 0.6 fusion.83
  99.8 2.8 fusion.17
  102.6 14.6 %all-gather.4.cloned.1.call-done = bf16[8,1,8,64,128]{4,3,2,1,0:T(8,128)(2,1)} async-done(((bf16[1,1,8,64,128]{4,3,2,1,0:T(8,128)(2,1)}), bf16[8,1,8,64,128]{4,3,2,1,0:T(8,128)(2,1)}) %all-gather.4.cloned.1.call-update) | async-done | bytes 1048592 | tf_op jit(solution)/shard_map/all_gather | solution.py:52
  117.2 2.1 fusion.63
  119.3 0.6 fusion.16
  121.7 1.2 convolution_convert_fusion
  123.0 25.6 %all_to_all.26 = bf16[8,384,256]{2,1,0:T(8,128)(2,1)S(1)} all-to-all(bf16[8,384,256]{2,1,0:T(8,128)(2,1)S(1)} %bitcast.262), channel_id=1, replica_groups=mesh['sp_0'=8,'sp_1'=8,'tp'=8] {'tp'}, dimensions={0} | all-to-all | bytes 3145728 | tf_op jit(solution)/shard_map/all_to_all | solution.py:74
  148.9 0.7 copy-done.12
  149.7 7.7 %all_to_all.27 = f32[8,1,384]{2,1,0:T(1,128)S(1)} all-to-all(f32[8,1,384]{2,1,0:T(1,128)S(1)} %broadcast_in_dim.53), channel_id=1, replica_groups=mesh['sp_0'=8,'sp_1'=8,'tp'=8] {'tp'}, dimensions={0} | all-to-all | bytes 24576 | tf_op jit(solution)/shard_map/all_to_all | solution.py:80
  157.8 1.3 broadcast_in_dim.54
  159.1 4.6 %all-to-all-start.2 = ((bf16[8,384,256]{1,2,0:T(8,128)(2,1)}), bf16[8,384,256]{1,2,0:T(8,128)(2,1)}, u32[]{:S(2)}, u32[]{:S(2)}) async-start(bf16[8,384,256]{1,2,0:T(8,128)(2,1)} %broadcast_in_dim.54), calls=%async_computation.2 | async-start | bytes 3145728 | tf_op jit(solution)/shard_map/all_to_all | solution.py:80
  163.8 21.3 %all-to-all-done.2 = bf16[8,384,256]{1,2,0:T(8,128)(2,1)} async-done(((bf16[8,384,256]{1,2,0:T(8,128)(2,1)}), bf16[8,384,256]{1,2,0:T(8,128)(2,1)}, u32[]{:S(2)}, u32[]{:S(2)}) %all-to-all-start.2) | async-done | bytes 1572896 | tf_op jit(solution)/shard_map/all_to_all | solution.py:80
  185.1 1.1 stack.2
  186.2 211.2 %all_to_all.28 = bf16[64,32,2048]{2,1,0:T(8,128)(2,1)} all-to-all(bf16[64,32,2048]{2,1,0:T(8,128)(2,1)S(1)} %stack.2), channel_id=1, replica_groups=mesh['sp_0'=8,'sp_1'=8,'tp'=8] {'sp_0','sp_1'}, dimensions={0} | all-to-all | bytes 16777216 | tf_op jit(solution)/shard_map/all_to_all | solution.py:22
  397.4 8.5 %fusion.4 = bf16[384,2048]{1,0:T(8,128)(2,1)} fusion(bf16[2048,2048]{1,0:T(8,128)(2,1)} %bitcast.261, bf16[384,2048]{0,1:T(8,128)(2,1)} %bitcast.64), kind=kOutput, calls=%fused_computation.6 | convolution fusion | flops 3223191552 | bytes 11534336 | tf_op jit(solution)/shard_map/dot_general | solution.py:204
  405.9 1.5 copy.160
  407.4 24.0 %all_to_all.29 = bf16[8,384,256]{2,1,0:T(8,128)(2,1)S(1)} all-to-all(bf16[8,384,256]{2,1,0:T(8,128)(2,1)S(1)} %bitcast.263), channel_id=1, replica_groups=mesh['sp_0'=8,'sp_1'=8,'tp'=8] {'tp'}, dimensions={0} | all-to-all | bytes 3145728 | tf_op jit(solution)/shard_map/all_to_all | solution.py:74
  431.7 0.7 fusion.47
  (124 shorter events, 7.3 us)
Async XLA Ops:
  6.5 115.2 %copy-start = (bf16[512,2048]{1,0:T(8,128)(2,1)S(1)}, bf16[512,2048]{1,0:T(8,128)(2,1)}, u32[]{:S(2)}) copy-start(bf16[512,2048]{1,0:T(8,128)(2,1)} %param.23) | copy-start | bytes 6291460
  6.5 12.9 %copy-start.7 = (bf16[384,512]{1,0:T(8,128)(2,1)S(1)}, bf16[384,512]{1,0:T(8,128)(2,1)}, u32[]{:S(2)}) copy-start(bf16[384,512]{1,0:T(8,128)(2,1)} %param.14) | copy-start | bytes 1179652
  6.5 67.3 %all-gather.6.cloned.1.call-start = ((), (), s32[]{:S(2)}) async-start(), calls=%async_computation.6 | async-start | bytes 1179648 | tf_op jit(solution)/shard_map/all_gather | solution.py:52
  8.9 12.1 %collective-permute-start = (bf16[3,768]{0,1:T(8,128)(2,1)}, bf16[3,768]{0,1:T(8,128)(2,1)S(1)}, u32[]{:S(2)}, u32[]{:S(2)}) collective-permute-start(bf16[3,768]{0,1:T(8,128)(2,1)} %copy.96), channel_id=1, source_target_pairs={{0,8},{8,16},{16,24},{24,32},{32,40},{40,48},{48,56},{56,64},{64,7... | collective-permute-start | bytes 13832 | tf_op jit(solution)/shard_map/ppermute | solution.py:37
  15.4 4.0 copy-start.16
  16.0 3.4 copy-start.18
  21.0 0.7 copy-start.11
  23.6 1.5 slice-start
  23.6 2.7 copy-start.28
  23.6 2.7 copy-start.29
  23.6 2.7 copy-start.30
  23.6 2.7 copy-start.31
  25.2 2.1 copy-start.13
  27.3 2.6 copy-start.2
  27.3 2.1 copy-start.32
  28.5 2.3 copy-start.37
  28.7 0.7 copy-start.9
  29.5 47.4 %copy-start.17 = (f32[3,1,8]{2,1,0:T(1,128)S(1)}, f32[3,1,8]{2,1,0:T(1,128)}, u32[]{:S(2)}) copy-start(f32[3,1,8]{2,1,0:T(1,128)} %copy-done.16) | copy-start | bytes 292
  29.5 47.4 %copy-start.8 = (bf16[384,512]{1,0:T(8,128)(2,1)S(1)}, bf16[384,512]{1,0:T(8,128)(2,1)}, u32[]{:S(2)}) copy-start(bf16[384,512]{1,0:T(8,128)(2,1)} %param.16) | copy-start | bytes 1179652
  30.0 47.8 %copy-start.19 = (f32[3,1,1,8]{3,2,1,0:T(1,128)S(1)}, f32[3,1,1,8]{3,2,1,0:T(1,128)}, u32[]{:S(2)}) copy-start(f32[3,1,1,8]{3,2,1,0:T(1,128)} %copy-done.18) | copy-start | bytes 292
  30.0 49.2 %copy-start.20 = (f32[3,1,1,8]{3,2,1,0:T(1,128)S(1)}, f32[3,1,1,8]{3,2,1,0:T(1,128)}, u32[]{:S(2)}) copy-start(f32[3,1,1,8]{3,2,1,0:T(1,128)} %get-tuple-element.13) | copy-start | bytes 292
  30.0 49.8 %copy-start.6 = (f32[3,128,8]{2,1,0:T(8,128)S(1)}, f32[3,128,8]{2,1,0:T(8,128)}, u32[]{:S(2)}) copy-start(f32[3,128,8]{2,1,0:T(8,128)} %get-tuple-element.11) | copy-start | bytes 36868
  30.0 69.4 %copy-start.3 = (f32[384,1,128]{2,1,0:T(1,128)S(1)}, f32[384,1,128]{2,1,0:T(1,128)}, u32[]{:S(2)}) copy-start(f32[384,1,128]{2,1,0:T(1,128)} %copy-done.2) | copy-start | bytes 589828
  30.7 86.5 %all-gather.4.cloned.1.call-start = ((), (), s32[]{:S(2)}) async-start(), calls=%async_computation.5 | async-start | bytes 1179648 | tf_op jit(solution)/shard_map/all_gather | solution.py:52
  44.7 54.9 %copy-start.27 = (f32[8]{0:T(128)}, f32[8]{0:T(128)S(1)}, u32[]{:S(2)}) copy-start(f32[8]{0:T(128)S(1)} %get-tuple-element.25) | copy-start | bytes 100
  44.7 54.9 %copy-start.21 = (f32[8]{0:T(128)}, f32[8]{0:T(128)S(1)}, u32[]{:S(2)}) copy-start(f32[8]{0:T(128)S(1)} %get-tuple-element.27) | copy-start | bytes 100
  44.7 54.9 %copy-start.22 = (f32[8]{0:T(128)}, f32[8]{0:T(128)S(1)}, u32[]{:S(2)}) copy-start(f32[8]{0:T(128)S(1)} %get-tuple-element.28) | copy-start | bytes 100
  44.7 54.9 %copy-start.23 = (f32[8]{0:T(128)}, f32[8]{0:T(128)S(1)}, u32[]{:S(2)}) copy-start(f32[8]{0:T(128)S(1)} %get-tuple-element.29) | copy-start | bytes 100
  44.7 54.9 %copy-start.24 = (f32[8]{0:T(128)}, f32[8]{0:T(128)S(1)}, u32[]{:S(2)}) copy-start(f32[8]{0:T(128)S(1)} %get-tuple-element.30) | copy-start | bytes 100
  44.7 54.9 %copy-start.25 = (f32[8]{0:T(128)}, f32[8]{0:T(128)S(1)}, u32[]{:S(2)}) copy-start(f32[8]{0:T(128)S(1)} %get-tuple-element.31) | copy-start | bytes 100
  44.7 54.9 %copy-start.26 = (f32[8]{0:T(128)}, f32[8]{0:T(128)S(1)}, u32[]{:S(2)}) copy-start(f32[8]{0:T(128)S(1)} %get-tuple-element.32) | copy-start | bytes 100
  99.7 17.5 %copy-start.1 = (bf16[64,64,128]{2,1,0:T(8,128)(2,1)S(1)}, bf16[64,64,128]{2,1,0:T(8,128)(2,1)}, u32[]{:S(2)}) copy-start(bf16[64,64,128]{2,1,0:T(8,128)(2,1)} %all-gather.6.cloned.1.call-done) | copy-start | bytes 3145732
  102.6 16.7 %copy-start.33 = (f32[3,8]{0,1:T(8,128)S(1)}, f32[3,8]{0,1:T(8,128)}, u32[]{:S(2)}) copy-start(f32[3,8]{0,1:T(8,128)} %copy.112) | copy-start | bytes 292
  102.6 16.7 %copy-start.34 = (f32[3,8]{0,1:T(8,128)S(1)}, f32[3,8]{0,1:T(8,128)}, u32[]{:S(2)}) copy-start(f32[3,8]{0,1:T(8,128)} %copy.110) | copy-start | bytes 292
  102.6 16.8 %copy-start.35 = (f32[3,1,1,8]{0,3,2,1:T(8,128)S(1)}, f32[3,1,1,8]{0,3,2,1:T(8,128)}, u32[]{:S(2)}) copy-start(f32[3,1,1,8]{0,3,2,1:T(8,128)} %copy.125) | copy-start | bytes 292
  102.6 16.8 %copy-start.39 = (pred[3,3]{1,0:T(4,128)(4,1)S(1)}, pred[3,3]{1,0:T(4,128)(4,1)}, u32[]{:S(2)}) copy-start(pred[3,3]{1,0:T(4,128)(4,1)} %iota_compare_fusion.1) | copy-start | bytes 31
  117.2 2.1 copy-start.10
  119.3 1.1 copy-start.5
  120.4 1.0 copy-start.4
  120.7 1.0 copy-start.38
  148.6 0.9 copy-start.12
  148.6 8.8 %copy-start.36 = (f32[256]{0:T(256)S(1)}, f32[256]{0:T(256)}, u32[]{:S(2)}) copy-start(f32[256]{0:T(256)} %param.25) | copy-start | bytes 3076
  159.1 4.6 %copy-start.14 = (bf16[1024,32]{0,1:T(8,128)(2,1)S(1)}, bf16[1024,32]{0,1:T(8,128)(2,1)}, u32[]{:S(2)}) copy-start(bf16[1024,32]{0,1:T(8,128)(2,1)} %param.27) | copy-start | bytes 196612
  159.1 4.7 %copy-start.15 = (bf16[32,1024]{1,0:T(8,128)(2,1)S(1)}, bf16[32,1024]{1,0:T(8,128)(2,1)}, u32[]{:S(2)}) copy-start(bf16[32,1024]{1,0:T(8,128)(2,1)} %param.26) | copy-start | bytes 196612
  159.1 26.0 %all-to-all-start.2 = ((bf16[8,384,256]{1,2,0:T(8,128)(2,1)}), bf16[8,384,256]{1,2,0:T(8,128)(2,1)}, u32[]{:S(2)}, u32[]{:S(2)}) async-start(bf16[8,384,256]{1,2,0:T(8,128)(2,1)} %broadcast_in_dim.54), calls=%async_computation.2 | async-start | bytes 3145728 | tf_op jit(solution)/shard_map/all_to_all | solution.py:80
Sparse Core Ops, SparseCore 0:
  30.8 43.0 all-gather.5
  76.3 40.9 all-gather.3
